TPU v7x, 32 devices: a whole 2x2x4 slice. The times are simulated.
32 devices in a mesh: ep: 8 (over z, x), tp: 4 (over y, core).
Axes of the slice: x: 2, y: 2, z: 4, core: 2. Of those that a mesh axis runs over, the one named last changes fastest.
Arguments:
- mix_bgate: bfloat16 [2048, 1024], P('ep', 'tp'), may hold values from -6 to 6
- mix_cgate: bfloat16 [2048, 1024], P('ep', 'tp'), may hold values from -6 to 6
- mix_input: bfloat16 [2048, 1024], P('ep', 'tp'), may hold values from -6 to 6
- conv_taps: float32 [3, 1024], P(None, 'tp'), may hold values from -3.5 to 3.5
- mix_out_w: bfloat16 [1024, 2048], P('tp'), may hold values from -0.1875 to 0.1875
- moe_x: bfloat16 [2048, 2048], P('ep', 'tp'), may hold values from -6 to 6
- moe_gain: float32 [2048], replicated, may hold values from 0.1 to 1.9
- routes: int32 [2048, 2], P('ep'), may hold values from 0 to 7, all different within a row; in each aligned block of 256 rows (0 to 255, 256 to 511, ...) at most 96 rows name the same one
- route_w: float32 [2048, 2], P('ep'), may hold values from 0.2 to 1
- w_gate: bfloat16 [8, 2048, 3584], P('ep', None, 'tp'), may hold values from -0.125 to 0.125
- w_up: bfloat16 [8, 2048, 3584], P('ep', None, 'tp'), may hold values from -0.125 to 0.125
- w_down: bfloat16 [8, 3584, 2048], P('ep', 'tp'), may hold values from -0.09375 to 0.09375
Outputs:
- mixed: bfloat16 [2048, 2048], P(('ep', 'tp'))
- routed: bfloat16 [2048, 2048], P('ep', 'tp')
Inputs may be any that keep to these rules, and one draw needn't show every extreme that they name: `routes`: among the 256 rows of one index of ep, each row names 2 different experts and no expert is named by more than 96 rows; in every draw some expert is named by exactly 96 rows of some index.
All inputs are finite; a program needn't handle non-finite values.
Results may differ from a plain program's by a relative error of at most 0.012.
Values may be sent and summed in bfloat16 or wider, within the bound.
A program may use at most 64 MiB of HBM per device.

v0:
```python
import jax
import jax.numpy as jnp
from jax import lax
from jax.sharding import PartitionSpec as P


def shifted(block, axis, distance):
    devices = range(lax.axis_size(axis))
    route = [(i - distance, i) for i in devices if i - distance in devices]
    return lax.ppermute(block, axis, route)


def rms_rows(values, gain):
    wide = values.astype(jnp.float32)
    scale = lax.rsqrt(jnp.mean(wide * wide, axis=-1, keepdims=True) + 1e-06)
    return (wide * scale * gain).astype(jnp.bfloat16)


def conv_mixer(mix_bgate, mix_cgate, mix_input, conv_taps, mix_out_w):
    length = mix_input.shape[0]
    reach = conv_taps.shape[0] - 1
    tail = jnp.stack([mix_cgate[length - reach :], mix_input[length - reach :]])
    before = shifted(tail, "ep", 1)
    gates_c = jnp.concatenate([before[0], mix_cgate], 0).astype(jnp.float32)
    inputs_h = jnp.concatenate([before[1], mix_input], 0).astype(jnp.float32)
    prod = gates_c * inputs_h
    conv = conv_taps[0] * prod[0:length]
    for j in range(1, reach + 1):
        conv = conv + conv_taps[j] * prod[j : j + length]
    gated = (mix_bgate.astype(jnp.float32) * conv).astype(jnp.bfloat16)
    return lax.psum_scatter(
        jnp.dot(gated, mix_out_w, preferred_element_type=jnp.float32).astype(jnp.bfloat16),
        "tp",
        scatter_dimension=0,
        tiled=True,
    )


def expert_layer(moe_x, moe_gain, routes, route_w, w_gate, w_up, w_down):
    whole = lax.all_gather(moe_x, "tp", axis=1, tiled=True)
    normed = rms_rows(whole, moe_gain)
    ntok, width = normed.shape
    top = routes.shape[1]
    n_ep = lax.axis_size("ep")
    n_tp = lax.axis_size("tp")
    per_dev = w_gate.shape[0]
    experts = per_dev * n_ep
    cap = 4 * ((3 * ntok * top + 8 * experts - 1) // (8 * experts))
    flat = routes.reshape(-1)
    onehot = (flat[:, None] == jnp.arange(experts, dtype=jnp.int32)[None, :]).astype(jnp.int32)
    earlier = jnp.cumsum(onehot, axis=0) - onehot
    slot = jnp.sum(earlier * onehot, axis=1)
    place = flat * cap + slot
    source = (
        jnp.full((experts * cap,), ntok, jnp.int32)
        .at[place]
        .set(jnp.arange(ntok * top, dtype=jnp.int32) // top)
    )
    padded = jnp.concatenate([normed, jnp.zeros((1, width), jnp.bfloat16)], 0)
    outgoing = padded[source].reshape(n_ep, per_dev, cap, width)
    part = cap // n_tp
    mine = lax.dynamic_slice_in_dim(outgoing, lax.axis_index("tp") * part, part, 2)
    landed = lax.all_to_all(mine, "ep", split_axis=0, concat_axis=0, tiled=True)
    arrived = lax.all_gather(landed, "tp", axis=2, tiled=True)
    gate = jnp.einsum("secd,edf->secf", arrived, w_gate, preferred_element_type=jnp.float32)
    upper = jnp.einsum("secd,edf->secf", arrived, w_up, preferred_element_type=jnp.float32)
    hidden = (jax.nn.silu(gate) * upper).astype(jnp.bfloat16)
    down = jnp.einsum("secf,efd->secd", hidden, w_down, preferred_element_type=jnp.float32)
    summed = lax.psum_scatter(down.astype(jnp.bfloat16), "tp", scatter_dimension=3, tiled=True)
    returned = lax.all_to_all(summed, "ep", split_axis=0, concat_axis=0, tiled=True)
    flat_back = returned.reshape(experts * cap, width // n_tp)
    picked = flat_back[place].astype(jnp.float32).reshape(ntok, top, width // n_tp)
    return jnp.sum(picked * route_w[:, :, None], axis=1).astype(jnp.bfloat16)


def body(
    mix_bgate,
    mix_cgate,
    mix_input,
    conv_taps,
    mix_out_w,
    moe_x,
    moe_gain,
    routes,
    route_w,
    w_gate,
    w_up,
    w_down,
):
    mixed = conv_mixer(mix_bgate, mix_cgate, mix_input, conv_taps, mix_out_w)
    routed = expert_layer(moe_x, moe_gain, routes, route_w, w_gate, w_up, w_down)
    return (mixed, routed)


def solution(mesh):
    in_specs = (
        P("ep", "tp"),
        P("ep", "tp"),
        P("ep", "tp"),
        P(None, "tp"),
        P("tp", None),
        P("ep", "tp"),
        P(),
        P("ep", None),
        P("ep", None),
        P("ep", None, "tp"),
        P("ep", None, "tp"),
        P("ep", "tp", None),
    )
    out_specs = (P(("ep", "tp"), None), P("ep", "tp"))
    return jax.shard_map(body, mesh=mesh, in_specs=in_specs, out_specs=out_specs, check_vma=False)
```

profile of v0, /device:TPU:0, one launch (start us, length us, event | category | flops | bytes accessed | tf_op | source)
XLA Modules:
  0.0 185.2 jit_solution(3375936974495529147)
XLA Ops:
  7.2 0.7 all-gather.3.cloned.1.call-update
  8.0 0.8 copy.20
  9.1 1.1 reduce-window.6
  10.5 0.7 broadcast_multiply_fusion
  11.6 2.4 %scatter_custom_fusion = s32[768]{0:T(1024)S(1)} fusion(s32[512]{0:T(512)S(1)} %bitcast.108, s32[512]{0:T(512)S(1)} %add_select_fusion, s32[]{:T(128)} %constant.40.clone.1), kind=kCustom, calls=%fused_computation.57 | custom fusion | bytes 3076 | tf_op jit(solution)/shard_map/scatter | solution.py:57
  14.1 15.0 %all-gather.3.cloned.1.call-done = bf16[256,2048]{1,0:T(8,128)(2,1)} async-done(((bf16[256,512]{1,0:T(8,128)(2,1)}), bf16[256,2048]{1,0:T(8,128)(2,1)}) %all-gather.3.cloned.1.call-update) | async-done | bytes 1048592 | tf_op jit(solution)/shard_map/all_gather | solution.py:40
  29.0 1.5 fusion.18
  30.6 1.5 fusion.20
  32.2 4.3 %gather_fusion = bf16[768,2048]{1,0:T(8,128)(2,1)} fusion(bf16[257,2048]{1,0:T(8,128)(2,1)S(1)} %concatenate.11, s32[1024]{0:T(1024)S(1)} %pad_clamp_fusion.1), kind=kCustom, calls=%fused_computation | custom fusion | bytes 6294528 | tf_op jit(solution)/shard_map/gather | solution.py:60
  36.5 1.2 constant_dynamic-slice_fusion
  37.7 25.9 %all_to_all.10 = bf16[8,1,24,2048]{3,2,1,0:T(8,128)(2,1)} all-to-all(bf16[8,1,24,2048]{3,2,1,0:T(8,128)(2,1)S(1)} %constant_dynamic-slice_fusion), channel_id=1, replica_groups=mesh['ep'=8,'tp'=4] {'ep'}, dimensions={0} | all-to-all | bytes 1572864 | tf_op jit(solution)/shard_map/all_to_all | solution.py:63
  63.7 26.7 %all-gather.5.cloned.1.call-done = bf16[8,1,96,2048]{3,2,0,1:T(8,128)(2,1)} async-done(((bf16[8,1,24,2048]{3,2,0,1:T(8,128)(2,1)}), bf16[8,1,96,2048]{3,2,0,1:T(8,128)(2,1)}) %all-gather.5.cloned.1.call-update) | async-done | bytes 3145744 | tf_op jit(solution)/shard_map/all_gather | solution.py:64
  90.4 8.0 %fusion.4 = f32[8,96,896]{2,1,0:T(8,128)} fusion(bf16[1,2048,896]{2,1,0:T(8,128)(2,1)} %param.21, bf16[8,1,96,2048]{3,2,0,1:T(8,128)(2,1)} %all-gather.5.cloned.1.call-done), kind=kOutput, calls=%fused_computation.7 | convolution fusion | flops 2818572288 | bytes 9568256 | tf_op jit(solution)/shard_map/secd,edf->secf/dot_general | solution.py:65
  98.4 12.1 %fusion.11 = bf16[8,1,96,2048]{3,2,0,1:T(8,128)(2,1)} fusion(bf16[1,896,2048]{2,1,0:T(8,128)(2,1)} %param.23, bf16[1,2048,896]{2,1,0:T(8,128)(2,1)} %param.22, bf16[8,1,96,2048]{3,2,0,1:T(8,128)(2,1)} %all-gather.5.cloned.1.call-done, f32[8,96,896]{2,1,0:T(8,128)} %fusion.4), kind=kOutput, calls=%fused_computation.12 | convolution fusion | flops 5642846208 | bytes 16384000 | tf_op jit(solution)/shard_map/secf,efd->secd/dot_general | solution.py:68
  110.6 0.8 copy-done.1
  111.5 3.4 %collective-permute-start = (bf16[2,2,256]{2,1,0:T(2,128)(2,1)S(1)}, bf16[2,2,256]{2,1,0:T(2,128)(2,1)S(1)}, u32[]{:S(2)}, u32[]{:S(2)}) collective-permute-start(bf16[2,2,256]{2,1,0:T(2,128)(2,1)S(1)} %pad_maximum_fusion), channel_id=1, source_target_pairs={{0,4},{4,8},{8,12},{12,16},{16,20},{20,24},{24,28},{1,5},{5,9},{9,... | collective-permute-start | bytes 6152 | tf_op jit(solution)/shard_map/ppermute | solution.py:10
  114.9 1.3 collective-permute-done
  116.2 1.5 convolution_convert_fusion
  117.7 30.7 %reduce-scatter.5.cloned.1.call-done = bf16[8,1,96,512]{3,2,0,1:T(8,128)(2,1)} async-done(((bf16[8,1,96,2048]{3,2,0,1:T(8,128)(2,1)}), bf16[8,1,96,512]{3,2,0,1:T(8,128)(2,1)}) %reduce-scatter.5.cloned.1.call-update) | async-done | bytes 786448 | tf_op jit(solution)/shard_map/reduce_scatter | solution.py:69
  148.4 5.5 %all-to-all-start.1 = ((bf16[8,1,96,512]{3,2,1,0:T(8,128)(2,1)}), bf16[8,1,96,512]{3,2,1,0:T(8,128)(2,1)S(1)}, u32[]{:S(2)}, u32[]{:S(2)}) async-start(bf16[8,1,96,512]{3,2,1,0:T(8,128)(2,1)} %bitcast.107), calls=%async_computation.3 | async-start | bytes 1572864 | tf_op jit(solution)/shard_map/all_to_all | solution.py:70
  154.1 19.9 %all-to-all-done.1 = bf16[8,1,96,512]{3,2,1,0:T(8,128)(2,1)S(1)} async-done(((bf16[8,1,96,512]{3,2,1,0:T(8,128)(2,1)}), bf16[8,1,96,512]{3,2,1,0:T(8,128)(2,1)S(1)}, u32[]{:S(2)}, u32[]{:S(2)}) %all-to-all-start.1) | async-done | bytes 786464 | tf_op jit(solution)/shard_map/all_to_all | solution.py:70
  174.0 2.0 %gather_fusion.1 = bf16[512,512]{1,0:T(8,128)(2,1)S(1)} fusion(bf16[768,512]{1,0:T(8,128)(2,1)S(1)} %bitcast.104, s32[1024]{0:T(1024)S(1)} %pad_clamp_fusion), kind=kCustom, calls=%fused_computation.1 | custom fusion | bytes 1050624 | tf_op jit(solution)/shard_map/gather | solution.py:72
  176.0 0.7 reshape.98
  176.6 2.1 %multiply_reduce_fusion = bf16[256,512]{1,0:T(8,128)(2,1)} fusion(f32[256,2,512]{2,1,0:T(2,128)S(1)} %reshape.98, f32[256,2]{1,0:T(8,128)S(1)} %copy.25), kind=kLoop, calls=%fused_computation.27 | loop fusion | flops 393216 | bytes 1312768 | tf_op jit(solution)/shard_map/reduce_sum | solution.py:73
  (41 shorter events, 1.6 us)
Async XLA Ops:
  7.2 109.1 %copy-start = (bf16[256,2048]{1,0:T(8,128)(2,1)S(1)}, bf16[256,2048]{1,0:T(8,128)(2,1)}, u32[]{:S(2)}) copy-start(bf16[256,2048]{1,0:T(8,128)(2,1)} %param.16) | copy-start | bytes 3145732
  7.2 21.9 %all-gather.3.cloned.1.call-start = ((), (), s32[]{:S(2)}) async-start(), calls=%async_computation.5 | async-start | bytes 1310720 | tf_op jit(solution)/shard_map/all_gather | solution.py:40
  7.9 82.5 %all-gather.5.cloned.1.call-start = ((), (), s32[]{:S(2)}) async-start(), calls=%async_computation.6 | async-start | bytes 3932160 | tf_op jit(solution)/shard_map/all_gather | solution.py:64
  63.6 84.8 %reduce-scatter.5.cloned.1.call-start = ((), (), s32[]{:S(2)}) async-start(), calls=%async_computation.7 | async-start | bytes 3932160 | tf_op jit(solution)/shard_map/reduce_scatter | solution.py:69
  110.5 0.9 copy-start.1
  110.5 1.0 copy-start.2
  110.5 4.4 %copy-start.4 = (f32[3,256]{1,0:T(4,128)S(1)}, f32[3,256]{1,0:T(4,128)}, u32[]{:S(2)}) copy-start(f32[3,256]{1,0:T(4,128)} %param.15) | copy-start | bytes 9220
  110.5 5.7 %copy-start.3 = (bf16[256,256]{1,0:T(8,128)(2,1)S(1)}, bf16[256,256]{1,0:T(8,128)(2,1)}, u32[]{:S(2)}) copy-start(bf16[256,256]{1,0:T(8,128)(2,1)} %param.12) | copy-start | bytes 393220
  110.5 43.4 %copy-start.5 = (f32[256,2]{0,1:T(2,128)S(1)}, f32[256,2]{0,1:T(2,128)}, u32[]{:S(2)}) copy-start(f32[256,2]{0,1:T(2,128)} %param.20) | copy-start | bytes 6148
  110.5 68.1 %reduce-scatter.3.cloned.1.call-start = ((), (), s32[]{:S(2)}) async-start(), calls=%async_computation.4 | async-start | bytes 1310720 | tf_op jit(solution)/shard_map/reduce_scatter | solution.py:31
  111.5 4.7 %collective-permute-start = (bf16[2,2,256]{2,1,0:T(2,128)(2,1)S(1)}, bf16[2,2,256]{2,1,0:T(2,128)(2,1)S(1)}, u32[]{:S(2)}, u32[]{:S(2)}) collective-permute-start(bf16[2,2,256]{2,1,0:T(2,128)(2,1)S(1)} %pad_maximum_fusion), channel_id=1, source_target_pairs={{0,4},{4,8},{8,12},{12,16},{16,20},{20,24},{24,28},{1,5},{5,9},{9,... | collective-permute-start | bytes 6152 | tf_op jit(solution)/shard_map/ppermute | solution.py:10
  148.4 25.6 %all-to-all-start.1 = ((bf16[8,1,96,512]{3,2,1,0:T(8,128)(2,1)}), bf16[8,1,96,512]{3,2,1,0:T(8,128)(2,1)S(1)}, u32[]{:S(2)}, u32[]{:S(2)}) async-start(bf16[8,1,96,512]{3,2,1,0:T(8,128)(2,1)} %bitcast.107), calls=%async_computation.3 | async-start | bytes 1572864 | tf_op jit(solution)/shard_map/all_to_all | solution.py:70
Sparse Core Ops, SparseCore 0:
  9.5 19.4 all-gather.2
  63.7 26.6 all-gather.4
  110.7 37.7 reduce-scatter.4
  151.4 24.7 reduce-scatter.2
where the time goes:
time: 186 us; the launch traced here: 185 us
  waiting for transfers between devices  94.3 us (51%)
  blocking collectives  25.9 us (14%)
  matrix products  21.5 us (12%)
  between operations  14 us (8%)
  local copies, waits for them, and re-layouts  13.3 us (7%)
  starting transfers between devices  9.05 us (5%)
  other arithmetic  7.18 us (4%)
    reduce_scatter x1, waiting for transfers between devices, expert_layer(): lax.psum_scatter(down.astype(jnp.bfloat16), 'tp', scatter_dimension=3, ti...  30.7 us
    all_gather x1, waiting for transfers between devices, expert_layer(): arrived = lax.all_gather(landed, 'tp', axis=2, tiled=True)  26.7 us
    all_to_all x1, blocking collectives, expert_layer(): landed = lax.all_to_all(mine, 'ep', split_axis=0, concat_axis=0, tiled=True)  25.9 us
    all_to_all x1, waiting for transfers between devices, expert_layer(): lax.all_to_all(summed, 'ep', split_axis=0, concat_axis=0, tiled=True)  19.9 us
    all_gather x1, waiting for transfers between devices, expert_layer(): whole = lax.all_gather(moe_x, 'tp', axis=1, tiled=True)  15 us
    dot_general x1, matrix products, expert_layer(): jnp.einsum('secf,efd->secd', hidden, w_down, preferred_element_type=jnp.f...  12.1 us
    dot_general x1, matrix products, expert_layer(): jnp.einsum('secd,edf->secf', arrived, w_gate, preferred_element_type=jnp....  8 us
    all_to_all x1, starting transfers between devices, expert_layer(): lax.all_to_all(summed, 'ep', split_axis=0, concat_axis=0, tiled=True)  5.52 us
  transfers between devices with their start and end apart: 6, of which 5 were waited for; matrix products, arithmetic and copies ran while one was open for 7% of the time, Pallas kernels for 0%

commit v1 on v0

v1 whole, which is shorter than its diff:
```python
import jax
import jax.numpy as jnp
from jax import lax
from jax.sharding import PartitionSpec as P


CHUNKS = 2


def shifted(block, axis, distance):
    devices = range(lax.axis_size(axis))
    route = [(i - distance, i) for i in devices if i - distance in devices]
    return lax.ppermute(block, axis, route)


def conv_mixer(mix_bgate, mix_cgate, mix_input, conv_taps, mix_out_w):
    length = mix_input.shape[0]
    reach = conv_taps.shape[0] - 1
    tail = jnp.stack([mix_cgate[length - reach :], mix_input[length - reach :]])
    before = shifted(tail, "ep", 1)
    gates_c = jnp.concatenate([before[0], mix_cgate], 0).astype(jnp.float32)
    inputs_h = jnp.concatenate([before[1], mix_input], 0).astype(jnp.float32)
    prod = gates_c * inputs_h
    conv = conv_taps[0] * prod[0:length]
    for j in range(1, reach + 1):
        conv = conv + conv_taps[j] * prod[j : j + length]
    gated = (mix_bgate.astype(jnp.float32) * conv).astype(jnp.bfloat16)
    return jnp.dot(gated, mix_out_w, preferred_element_type=jnp.float32).astype(jnp.bfloat16)


def chunk_edges(cap, count):
    base = cap // count
    return [(i * base, cap if i == count - 1 else (i + 1) * base) for i in range(count)]


def route_tables(routes, experts, cap):
    ntok, top = routes.shape
    chosen = routes[:, :, None] == jnp.arange(experts, dtype=jnp.int32)
    named = jnp.any(chosen, axis=1)
    row = lax.broadcasted_iota(jnp.int32, (ntok, ntok), 0)
    col = lax.broadcasted_iota(jnp.int32, (ntok, ntok), 1)
    rank = jnp.dot(
        (col < row).astype(jnp.bfloat16),
        named.astype(jnp.bfloat16),
        preferred_element_type=jnp.float32,
    ).astype(jnp.int32)
    return chosen, named, rank


def norm_rows(parts, gain):
    n_tp, rows, d = parts.shape
    wide = parts.astype(jnp.float32)
    total = jnp.sum(wide * wide, axis=(0, 2))
    scale = lax.rsqrt(total / (n_tp * d) + 1e-06)[:, None]
    pieces = [
        (wide[i] * scale * gain[i * d : (i + 1) * d]).astype(jnp.bfloat16) for i in range(n_tp)
    ]
    return jnp.concatenate(pieces, axis=1)


def experts_part(parts, moe_gain, w_gate, w_up, w_down):
    n_tp, n_ep, per_dev, c, d = parts.shape
    normed = norm_rows(parts.reshape(n_tp, n_ep * per_dev * c, d), moe_gain)
    normed = normed.reshape(n_ep, per_dev, c, n_tp * d)
    outs = []
    for e in range(per_dev):
        rows = normed[:, e].reshape(n_ep * c, n_tp * d)
        gate = jnp.dot(rows, w_gate[e], preferred_element_type=jnp.float32)
        upper = jnp.dot(rows, w_up[e], preferred_element_type=jnp.float32)
        hidden = (jax.nn.silu(gate) * upper).astype(jnp.bfloat16)
        down = jnp.dot(hidden, w_down[e], preferred_element_type=jnp.float32)
        outs.append(down.astype(jnp.bfloat16).reshape(n_ep, c, -1))
    return jnp.stack(outs, axis=1)


def body(
    mix_bgate,
    mix_cgate,
    mix_input,
    conv_taps,
    mix_out_w,
    moe_x,
    moe_gain,
    routes,
    route_w,
    w_gate,
    w_up,
    w_down,
):
    ntok, d = moe_x.shape
    top = routes.shape[1]
    n_ep = lax.axis_size("ep")
    n_tp = lax.axis_size("tp")
    per_dev = w_gate.shape[0]
    experts = per_dev * n_ep
    cap = 4 * ((3 * ntok * top + 8 * experts - 1) // (8 * experts))
    edges = chunk_edges(cap, CHUNKS)

    share = conv_mixer(mix_bgate, mix_cgate, mix_input, conv_taps, mix_out_w)
    share, moe_x = lax.optimization_barrier((share, moe_x))
    mixed = lax.psum_scatter(share, "tp", scatter_dimension=0, tiled=True)

    chosen, named, rank = route_tables(routes, experts, cap)
    landed = []
    for lo, hi in edges:
        slots = jnp.arange(lo, hi, dtype=jnp.int32)
        pick = named.T[:, None, :] & (rank.T[:, None, :] == slots[None, :, None])
        pick = pick.astype(jnp.bfloat16).reshape(experts * (hi - lo), ntok)
        out = jnp.dot(pick, moe_x, preferred_element_type=jnp.float32).astype(jnp.bfloat16)
        out = out.reshape(n_ep, per_dev, hi - lo, d)
        landed.append(lax.all_to_all(out, "ep", split_axis=0, concat_axis=0, tiled=True))
    gathered = [lax.all_gather(x, "tp", axis=0, tiled=False) for x in landed]
    returned = []
    down = None
    for parts in gathered:
        if down is not None:
            parts, down = lax.optimization_barrier((parts, down))
        down = experts_part(parts, moe_gain, w_gate, w_up, w_down)
        summed = lax.psum_scatter(down, "tp", scatter_dimension=3, tiled=True)
        returned.append(lax.all_to_all(summed, "ep", split_axis=0, concat_axis=0, tiled=True))
    total = jnp.zeros((top * ntok, d), jnp.float32)
    for (lo, hi), back in zip(edges, returned):
        slots = jnp.arange(lo, hi, dtype=jnp.int32)
        at = jnp.moveaxis(chosen, 1, 0)[:, :, :, None] & (rank[:, :, None] == slots)[None]
        at = at.astype(jnp.bfloat16).reshape(top * ntok, experts * (hi - lo))
        total = total + jnp.dot(
            at, back.reshape(experts * (hi - lo), d), preferred_element_type=jnp.float32
        )
    picked = total.reshape(top, ntok, d)
    routed = jnp.sum(picked * route_w.T[:, :, None], axis=0).astype(jnp.bfloat16)
    return (mixed, routed)


def solution(mesh):
    in_specs = (
        P("ep", "tp"),
        P("ep", "tp"),
        P("ep", "tp"),
        P(None, "tp"),
        P("tp", None),
        P("ep", "tp"),
        P(),
        P("ep", None),
        P("ep", None),
        P("ep", None, "tp"),
        P("ep", None, "tp"),
        P("ep", "tp", None),
    )
    out_specs = (P(("ep", "tp"), None), P("ep", "tp"))
    return jax.shard_map(body, mesh=mesh, in_specs=in_specs, out_specs=out_specs, check_vma=False)
```

time: 186 us -> 186 us (level)
  waiting for transfers between devices: 94.3 us -> 79.4 us
  matrix products: 21.5 us -> 29.1 us
  starting transfers between devices: 9.05 us -> 16.1 us
  local copies, waits for them, and re-layouts: 13.3 us -> 7.33 us
  blocking collectives: 25.9 us -> 31.3 us
    all_gather x2, waiting for transfers between devices: 41.7 us -> 20.9 us  [body(): gathered = [lax.all_gather(x, 'tp', axis=0, tiled=False) for x in landed]]
    reduce_scatter x2 -> x3, waiting for transfers between devices: 30.7 us -> 48 us  [the longest x2 38.7 us: body(): summed = lax.psum_scatter(down, 'tp', scatter_dimension=3, tiled=True)]
    all_to_all x1 -> x2, waiting for transfers between devices: 19.9 us -> 9.86 us  [body(): lax.all_to_all(summed, 'ep', split_axis=0, concat_axis=0, tiled=True)]
    dot_general x2 -> x9, matrix products: 20.1 us -> 26.7 us  [the longest x2 17.3 us: experts_part(): down = jnp.dot(hidden, w_down[e], preferred_element_type=jnp.float32)]
    gather x2 -> x0, local copies, waits for them, and re-layouts: 6.23 us -> none  [the longest x1 4.27 us: expert_layer(): outgoing = padded[source].reshape(n_ep, per_dev, cap, width)]
    all_to_all x1 -> x2, starting transfers between devices: 5.52 us -> 11 us  [body(): lax.all_to_all(summed, 'ep', split_axis=0, concat_axis=0, tiled=True)]
    all_to_all x1 -> x2, blocking collectives: 25.9 us -> 31.3 us  [body(): lax.all_to_all(out, 'ep', split_axis=0, concat_axis=0, tiled=True)]
    scatter x1 -> x0, local copies, waits for them, and re-layouts: 2.45 us -> none  [expert_layer(): source = jnp.full((experts * cap,), ntok, jnp.int32).at[place].set(jnp.ar...]
  transfers between devices with their start and end apart: 6 -> 8, of which waited for: 5 -> 6; matrix products, arithmetic and copies ran while one was open for 7% -> 12% of each run, Pallas kernels for 0% -> 0%
where the time goes in v1:
time: 186 us
  waiting for transfers between devices  79.4 us (43%)
  blocking collectives  31.3 us (17%)
  matrix products  29.1 us (16%)
  starting transfers between devices  16.1 us (9%)
  between operations  14.1 us (8%)
  other arithmetic  8.36 us (4%)
  local copies, waits for them, and re-layouts  7.33 us (4%)
    reduce_scatter x2, waiting for transfers between devices, body(): summed = lax.psum_scatter(down, 'tp', scatter_dimension=3, tiled=True)  38.7 us
    all_to_all x2, blocking collectives, body(): lax.all_to_all(out, 'ep', split_axis=0, concat_axis=0, tiled=True)  31.3 us
    all_gather x2, waiting for transfers between devices, body(): gathered = [lax.all_gather(x, 'tp', axis=0, tiled=False) for x in landed]  20.9 us
    dot_general x2, matrix products, experts_part(): down = jnp.dot(hidden, w_down[e], preferred_element_type=jnp.float32)  17.3 us
    all_to_all x2, starting transfers between devices, body(): lax.all_to_all(summed, 'ep', split_axis=0, concat_axis=0, tiled=True)  11 us
    all_to_all x2, waiting for transfers between devices, body(): lax.all_to_all(summed, 'ep', split_axis=0, concat_axis=0, tiled=True)  9.86 us
    reduce_scatter x1, waiting for transfers between devices, body(): mixed = lax.psum_scatter(share, 'tp', scatter_dimension=0, tiled=True)  9.36 us
    dot_general x2, matrix products, experts_part(): gate = jnp.dot(rows, w_gate[e], preferred_element_type=jnp.float32)  7.8 us
  transfers between devices with their start and end apart: 8, of which 6 were waited for; matrix products, arithmetic and copies ran while one was open for 12% of the time, Pallas kernels for 0%

profile of v1, /device:TPU:0, one launch (start us, length us, event | category | flops | bytes accessed | tf_op | source)
XLA Modules:
  0.0 185.7 jit_solution(15180672576071521467)
XLA Ops:
  7.2 0.8 slice_bitcast_fusion.2
  8.1 4.9 %collective-permute-start = (bf16[2,2,256]{2,1,0:T(2,128)(2,1)S(1)}, bf16[2,2,256]{2,1,0:T(2,128)(2,1)S(1)}, u32[]{:S(2)}, u32[]{:S(2)}) collective-permute-start(bf16[2,2,256]{2,1,0:T(2,128)(2,1)S(1)} %pad_maximum_fusion.8), channel_id=1, source_target_pairs={{0,4},{4,8},{8,12},{12,16},{16,20},{20,24},{24,28},{1,5},{5,9},{9,... | collective-permute-start | bytes 6152 | tf_op jit(solution)/shard_map/ppermute | solution.py:13
  15.0 1.0 convert_multiply_fusion
  16.1 2.4 %convolution_convert_fusion = bf16[256,2048]{1,0:T(8,128)(2,1)} fusion(bf16[256,2048]{1,0:T(8,128)(2,1)S(1)} %copy-done, f32[258,256]{1,0:T(8,128)S(1)} %convert_multiply_fusion, bf16[256,256]{1,0:T(8,128)(2,1)} %param.12, f32[256]{0:T(256)S(1)} %bitcast.159, f32[256]{0:T(256)S(1)} %bitcast.160, f32[256]{0:T(256)S(1)} %bitcast.158), kind=kOutput, calls=%fused_computation.16 | convolution fusion | flops 269484032 | bytes 3017728 | tf_op jit(solution)/shard_map/dot_general | solution.py:28
  18.8 16.6 %all_to_all.20 = bf16[8,1,48,512]{3,2,1,0:T(8,128)(2,1)} all-to-all(bf16[8,1,48,512]{3,2,1,0:T(8,128)(2,1)S(1)} %bitcast.147), channel_id=1, replica_groups=mesh['ep'=8,'tp'=4] {'ep'}, dimensions={0} | all-to-all | bytes 786432 | tf_op jit(solution)/shard_map/all_to_all | solution.py:111
  35.7 14.7 %all_to_all.21 = bf16[8,1,48,512]{3,2,1,0:T(8,128)(2,1)} all-to-all(bf16[8,1,48,512]{3,2,1,0:T(8,128)(2,1)S(1)} %bitcast.148), channel_id=1, replica_groups=mesh['ep'=8,'tp'=4] {'ep'}, dimensions={0} | all-to-all | bytes 786432 | tf_op jit(solution)/shard_map/all_to_all | solution.py:111
  50.5 3.3 %all-gather.7.cloned.1.call-done = bf16[32,1,48,512]{3,2,1,0:T(8,128)(2,1)} async-done(((bf16[8,1,48,512]{3,2,1,0:T(8,128)(2,1)}), bf16[32,1,48,512]{3,2,1,0:T(8,128)(2,1)}) %all-gather.7.cloned.1.call-update) | async-done | bytes 1572880 | tf_op jit(solution)/shard_map/all_gather | solution.py:112
  53.9 1.9 %multiply_reduce_fusion.1 = f32[8,48]{1,0:T(8,128)S(1)} fusion(bf16[4,8,1,48,512]{4,3,1,0,2:T(8,128)(2,1)} %bitcast.142), kind=kLoop, calls=%fused_computation.13 | loop fusion | flops 2358912 | bytes 1574400 | tf_op jit(solution)/shard_map/reduce_sum | solution.py:53
  55.9 1.6 fusion.69
  57.5 17.6 %all-gather.5.cloned.1.call-done = bf16[32,1,48,512]{3,2,1,0:T(8,128)(2,1)} async-done(((bf16[8,1,48,512]{3,2,1,0:T(8,128)(2,1)}), bf16[32,1,48,512]{3,2,1,0:T(8,128)(2,1)}) %all-gather.5.cloned.1.call-update) | async-done | bytes 1572880 | tf_op jit(solution)/shard_map/all_gather | solution.py:112
  75.1 1.9 %multiply_reduce_fusion = f32[32,48]{1,0:T(8,128)S(1)} fusion(bf16[32,1,48,512]{3,2,1,0:T(8,128)(2,1)} %all-gather.5.cloned.1.call-done), kind=kLoop, calls=%fused_computation.12 | loop fusion | flops 2357760 | bytes 1579008 | tf_op jit(solution)/shard_map/reduce_sum | solution.py:53
  80.5 0.8 copy-done.14
  81.3 2.9 %fusion.10 = f32[384,896]{1,0:T(8,128)} fusion(bf16[1,2048,896]{2,1,0:T(8,128)(2,1)S(1)} %copy-done.14, bf16[384,512]{1,0:T(8,128)(2,1)S(1)} %get-tuple-element.35, bf16[384,512]{1,0:T(8,128)(2,1)S(1)} %get-tuple-element.33, bf16[384,512]{1,0:T(8,128)(2,1)S(1)} %get-tuple-element.31, bf16[384,512]{1,0:T(8,128)(2,1)S(1)} %get-tuple-element.30), kind=kOutput, calls=%fused_computation.10 | convolution fusion | flops 1415577600 | bytes 6619136 | tf_op jit(solution)/shard_map/dot_general | solution.py:68
  84.2 8.6 %fusion.12 = bf16[384,2048]{1,0:T(8,128)(2,1)} fusion(bf16[1,896,2048]{2,1,0:T(8,128)(2,1)} %param.23, bf16[1,2048,896]{2,1,0:T(8,128)(2,1)} %param.22, f32[384,896]{1,0:T(8,128)} %fusion.10, bf16[384,512]{1,0:T(8,128)(2,1)} %copy-done.10, bf16[384,512]{1,0:T(8,128)(2,1)} %copy-done.9, bf16[384,512]{1,0:T(8,128)(2,1)} %copy-done.8, ...), kind=kOutput, calls=%fused_computation.14 | convolution fusion | flops 2827714560 | bytes 11862016 | tf_op jit(solution)/shard_map/dot_general | solution.py:71
  92.9 4.9 %fusion.8 = f32[384,896]{1,0:T(8,128)} fusion(bf16[1,2048,896]{2,1,0:T(8,128)(2,1)} %param.21, bf16[384,512]{1,0:T(8,128)(2,1)S(1)} %get-tuple-element.36, bf16[384,512]{1,0:T(8,128)(2,1)S(1)} %get-tuple-element.34, bf16[384,512]{1,0:T(8,128)(2,1)S(1)} %get-tuple-element.32, bf16[384,512]{1,0:T(8,128)(2,1)S(1)} %get-tuple-element.29), kind=kOutput, calls=%fused_computation.8 | convolution fusion | flops 1415577600 | bytes 6619136 | tf_op jit(solution)/shard_map/dot_general | solution.py:68
  97.8 8.6 %fusion.15 = bf16[384,2048]{1,0:T(8,128)(2,1)} fusion(bf16[1,896,2048]{2,1,0:T(8,128)(2,1)} %param.23, bf16[1,2048,896]{2,1,0:T(8,128)(2,1)} %param.22, f32[384,896]{1,0:T(8,128)} %fusion.8, bf16[384,512]{1,0:T(8,128)(2,1)S(1)} %get-tuple-element.36, bf16[384,512]{1,0:T(8,128)(2,1)S(1)} %get-tuple-element.34, bf16[384,512]{1,0:T(8,128)(2,1)S(1)} %get-tuple-element.32, ...), kind=kOutput, calls=%fused_computation.15 | convolution fusion | flops 2827714560 | bytes 11862016 | tf_op jit(solution)/shard_map/dot_general | solution.py:71
  107.1 13.9 %reduce-scatter.6.cloned.1.call-done = bf16[8,1,48,512]{3,2,1,0:T(8,128)(2,1)} async-done(((bf16[8,1,48,2048]{3,2,1,0:T(8,128)(2,1)}), bf16[8,1,48,512]{3,2,1,0:T(8,128)(2,1)}) %reduce-scatter.6.cloned.1.call-update) | async-done | bytes 393232 | tf_op jit(solution)/shard_map/reduce_scatter | solution.py:119
  121.0 5.5 %all-to-all-start.1 = ((bf16[8,1,48,512]{3,2,1,0:T(8,128)(2,1)}), bf16[8,1,48,512]{3,2,1,0:T(8,128)(2,1)S(1)}, u32[]{:S(2)}, u32[]{:S(2)}) async-start(bf16[8,1,48,512]{3,2,1,0:T(8,128)(2,1)} %reduce-scatter.6.cloned.1.call-done), calls=%async_computation.3 | async-start | bytes 786432 | tf_op jit(solution)/shard_map/all_to_all | solution.py:120
  126.6 24.8 %reduce-scatter.8.cloned.1.call-done = bf16[8,1,48,512]{3,2,1,0:T(8,128)(2,1)} async-done(((bf16[8,1,48,2048]{3,2,1,0:T(8,128)(2,1)}), bf16[8,1,48,512]{3,2,1,0:T(8,128)(2,1)}) %reduce-scatter.8.cloned.1.call-update) | async-done | bytes 393232 | tf_op jit(solution)/shard_map/reduce_scatter | solution.py:119
  151.4 5.5 %all-to-all-start.3 = ((bf16[8,1,48,512]{3,2,1,0:T(8,128)(2,1)}), bf16[8,1,48,512]{3,2,1,0:T(8,128)(2,1)S(1)}, u32[]{:S(2)}, u32[]{:S(2)}) async-start(bf16[8,1,48,512]{3,2,1,0:T(8,128)(2,1)} %reduce-scatter.8.cloned.1.call-done), calls=%async_computation.6 | async-start | bytes 786432 | tf_op jit(solution)/shard_map/all_to_all | solution.py:120
  156.9 1.0 broadcast_and_fusion
  158.6 9.9 %all-to-all-done.3 = bf16[8,1,48,512]{3,2,1,0:T(8,128)(2,1)S(1)} async-done(((bf16[8,1,48,512]{3,2,1,0:T(8,128)(2,1)}), bf16[8,1,48,512]{3,2,1,0:T(8,128)(2,1)S(1)}, u32[]{:S(2)}, u32[]{:S(2)}) %all-to-all-start.3) | async-done | bytes 393248 | tf_op jit(solution)/shard_map/all_to_all | solution.py:120
  169.0 0.8 multiply_reduce_fusion.2
  169.8 9.4 %reduce-scatter.4.cloned.1.call-done = bf16[64,2048]{1,0:T(8,128)(2,1)} async-done(((bf16[256,2048]{1,0:T(8,128)(2,1)}), bf16[64,2048]{1,0:T(8,128)(2,1)}) %reduce-scatter.4.cloned.1.call-update) | async-done | bytes 262160 | tf_op jit(solution)/shard_map/reduce_scatter | solution.py:101
  (68 shorter events, 8.3 us)
Async XLA Ops:
  7.2 8.9 %copy-start = (bf16[256,2048]{1,0:T(8,128)(2,1)S(1)}, bf16[256,2048]{1,0:T(8,128)(2,1)}, u32[]{:S(2)}) copy-start(bf16[256,2048]{1,0:T(8,128)(2,1)} %param.16) | copy-start | bytes 3145732
  7.2 11.3 %copy-start.6 = (bf16[256,512]{1,0:T(8,128)(2,1)S(1)}, bf16[256,512]{1,0:T(8,128)(2,1)}, u32[]{:S(2)}) copy-start(bf16[256,512]{1,0:T(8,128)(2,1)} %param.17) | copy-start | bytes 786436
  7.2 46.7 %all-gather.7.cloned.1.call-start = ((), (), s32[]{:S(2)}) async-start(), calls=%async_computation.11 | async-start | bytes 1966080 | tf_op jit(solution)/shard_map/all_gather | solution.py:112
  8.1 7.0 %collective-permute-start = (bf16[2,2,256]{2,1,0:T(2,128)(2,1)S(1)}, bf16[2,2,256]{2,1,0:T(2,128)(2,1)S(1)}, u32[]{:S(2)}, u32[]{:S(2)}) collective-permute-start(bf16[2,2,256]{2,1,0:T(2,128)(2,1)S(1)} %pad_maximum_fusion.8), channel_id=1, source_target_pairs={{0,4},{4,8},{8,12},{12,16},{16,20},{20,24},{24,28},{1,5},{5,9},{9,... | collective-permute-start | bytes 6152 | tf_op jit(solution)/shard_map/ppermute | solution.py:13
  18.5 32.0 %copy-start.12 = (f32[2048]{0:T(1024)S(1)}, f32[2048]{0:T(1024)}, u32[]{:S(2)}) copy-start(f32[2048]{0:T(1024)} %param.18) | copy-start | bytes 24580
  35.4 39.7 %all-gather.5.cloned.1.call-start = ((), (), s32[]{:S(2)}) async-start(), calls=%async_computation.10 | async-start | bytes 1966080 | tf_op jit(solution)/shard_map/all_gather | solution.py:112
  50.5 70.5 %reduce-scatter.6.cloned.1.call-start = ((), (), s32[]{:S(2)}) async-start(), calls=%async_computation.8 | async-start | bytes 1966080 | tf_op jit(solution)/shard_map/reduce_scatter | solution.py:119
  53.9 2.0 %copy-start.2 = (bf16[32,1,48,512]{3,2,1,0:T(8,128)(2,1)S(1)}, bf16[32,1,48,512]{3,2,1,0:T(8,128)(2,1)}, u32[]{:S(2)}) copy-start(bf16[32,1,48,512]{3,2,1,0:T(8,128)(2,1)} %all-gather.7.cloned.1.call-done) | copy-start | bytes 4718596
  75.1 2.0 %copy-start.1 = (bf16[32,1,48,512]{3,2,1,0:T(8,128)(2,1)S(1)}, bf16[32,1,48,512]{3,2,1,0:T(8,128)(2,1)}, u32[]{:S(2)}) copy-start(bf16[32,1,48,512]{3,2,1,0:T(8,128)(2,1)} %all-gather.5.cloned.1.call-done) | copy-start | bytes 4718596
  77.1 1.1 copy-start.3
  77.1 1.4 copy-start.4
  77.1 1.6 copy-start.5
  78.7 2.6 %copy-start.14 = (bf16[1,2048,896]{2,1,0:T(8,128)(2,1)S(1)}, bf16[1,2048,896]{2,1,0:T(8,128)(2,1)}, u32[]{:S(2)}) copy-start(bf16[1,2048,896]{2,1,0:T(8,128)(2,1)} %param.21) | copy-start | bytes 11010052
  79.4 0.8 copy-start.7
  79.4 0.9 copy-start.8
  79.4 1.0 copy-start.9
  79.4 1.1 copy-start.10
  92.8 58.5 %reduce-scatter.8.cloned.1.call-start = ((), (), s32[]{:S(2)}) async-start(), calls=%async_computation.9 | async-start | bytes 1966080 | tf_op jit(solution)/shard_map/reduce_scatter | solution.py:119
  106.5 50.4 %copy-start.11 = (s32[256,2]{0,1:T(2,128)S(1)}, s32[256,2]{0,1:T(2,128)}, u32[]{:S(2)}) copy-start(s32[256,2]{0,1:T(2,128)} %param.19) | copy-start | bytes 6148
  106.5 72.7 %reduce-scatter.4.cloned.1.call-start = ((), (), s32[]{:S(2)}) async-start(), calls=%async_computation.7 | async-start | bytes 1310720 | tf_op jit(solution)/shard_map/reduce_scatter | solution.py:101
  121.0 30.4 %all-to-all-start.1 = ((bf16[8,1,48,512]{3,2,1,0:T(8,128)(2,1)}), bf16[8,1,48,512]{3,2,1,0:T(8,128)(2,1)S(1)}, u32[]{:S(2)}, u32[]{:S(2)}) async-start(bf16[8,1,48,512]{3,2,1,0:T(8,128)(2,1)} %reduce-scatter.6.cloned.1.call-done), calls=%async_computation.3 | async-start | bytes 786432 | tf_op jit(solution)/shard_map/all_to_all | solution.py:120
  151.4 17.1 %all-to-all-start.3 = ((bf16[8,1,48,512]{3,2,1,0:T(8,128)(2,1)}), bf16[8,1,48,512]{3,2,1,0:T(8,128)(2,1)S(1)}, u32[]{:S(2)}, u32[]{:S(2)}) async-start(bf16[8,1,48,512]{3,2,1,0:T(8,128)(2,1)} %reduce-scatter.8.cloned.1.call-done), calls=%async_computation.6 | async-start | bytes 786432 | tf_op jit(solution)/shard_map/all_to_all | solution.py:120
  158.1 10.9 %copy-start.13 = (f32[256,2]{0,1:T(2,128)S(1)}, f32[256,2]{0,1:T(2,128)}, u32[]{:S(2)}) copy-start(f32[256,2]{0,1:T(2,128)} %param.20) | copy-start | bytes 6148
Sparse Core Ops, SparseCore 0:
  35.5 18.3 all-gather.6
  55.4 19.6 all-gather.4
  93.0 27.9 reduce-scatter.5
  123.4 27.9 reduce-scatter.7
  154.3 24.8 reduce-scatter.3
